TPU v7x, 1024 devices: a whole 8x8x8 slice. The times are simulated.
1024 devices in a mesh: fs: 64 (over z, y), tp: 16 (over x, core).
Axes of the slice: x: 8, y: 8, z: 8, core: 2. Of those that a mesh axis runs over, the one named last changes fastest.
Arguments:
- up_pre: bfloat16 [49152, 4096], P('fs', 'tp'), may hold values from -6 to 6
- gate_value: bfloat16 [49152, 4096], P('fs', 'tp'), may hold values from -6 to 6
- out_cotangent: bfloat16 [49152, 2048], P('fs', 'tp'), may hold values from -8 to 8
- down_weight: bfloat16 [2048, 4096], P('fs', 'tp'), may hold values from -0.09375 to 0.09375
- conv_weight: float32 [3, 4096], P(None, 'tp'), may hold values from -3.5 to 3.5
- conv_bias: float32 [4096], P('tp'), may hold values from -3 to 3
Outputs:
- up_grad: bfloat16 [49152, 4096], P('fs', 'tp')
- gate_grad: bfloat16 [49152, 4096], P('fs', 'tp')
- weight_grad: float32 [2048, 4096], P('fs', 'tp')
- tap_grad: float32 [3, 4096], P(None, 'tp')
- bias_grad: float32 [4096], P('tp')
- unit_norms: float32 [4096], P('tp')
All inputs are finite; a program needn't handle non-finite values.
Results may differ from a plain program's by a relative error of at most 0.0034.
Values may be sent and summed in bfloat16 or wider, within the bound.
A program may use at most 32 MiB of HBM per device.

v0:
```python
import jax
import jax.numpy as jnp
from jax import lax
from jax.sharding import Mesh
from jax.sharding import PartitionSpec as P

FS = ("fs_0", "fs_1")


def from_behind(value, axis, steps):
    count = lax.axis_size(axis)
    initial, last = (max(0, -steps), min(count, count - steps))
    return lax.ppermute(value, axis, [(source, source + steps) for source in range(initial, last)])


def joined_along(parts, dim):
    parts = jnp.moveaxis(parts, 0, dim)
    lengths = parts.shape
    return parts.reshape(*lengths[:dim], lengths[dim] * lengths[dim + 1], *lengths[dim + 2 :])


def from_everyone(value, axis):
    peers = lax.axis_size(axis)
    return lax.all_to_all(
        jnp.broadcast_to(value[None], (peers, *value.shape)), axis, 0, 0, tiled=True
    )


def gathered_copies(value, axis, dim):
    return joined_along(from_everyone(value, axis), dim)


def summed_rows(value, axes, dim):
    if not axes:
        return value
    nearer = lax.psum_scatter(value, axes[0], scatter_dimension=dim, tiled=True)
    return summed_rows(nearer, axes[1:], dim)


def one_axis_at_a_time(value, axes):
    for axis in axes:
        value = lax.psum(value, axis)
    return value


def per_device(up_pre, gate_value, out_cotangent, down_weight, conv_weight, conv_bias):
    tap_count = conv_weight.shape[0]
    tok_rows = up_pre.shape[0]
    before = from_behind(up_pre[tok_rows - (tap_count - 1) :], FS, 1)
    padded = jnp.concatenate([before, up_pre], 0).astype(jnp.float32)
    conv_out = jnp.zeros(up_pre.shape, jnp.float32) + conv_bias[None, :]
    for tap_index in range(tap_count):
        conv_out = (
            conv_out + conv_weight[tap_index][None, :] * padded[tap_index : tap_index + tok_rows]
        )
    sigmoid_val = jax.nn.sigmoid(conv_out)
    activated = conv_out * sigmoid_val
    gate_float = gate_value.astype(jnp.float32)
    hidden = (activated * gate_float).astype(jnp.bfloat16)
    full_cot = lax.all_gather(out_cotangent, "tp", axis=1, tiled=True)
    hidden_grad = jnp.dot(
        full_cot, gathered_copies(down_weight, FS, 0), preferred_element_type=jnp.float32
    )
    gate_grad = (hidden_grad * activated).astype(jnp.bfloat16)
    conv_grad = hidden_grad * gate_float * sigmoid_val * (1.0 + conv_out * (1.0 - sigmoid_val))
    after_rows = from_behind(conv_grad[: tap_count - 1], FS, -1)
    after = jnp.concatenate([conv_grad, after_rows], 0)
    up_grad = jnp.zeros(up_pre.shape, jnp.float32)
    for tap_index in range(tap_count):
        lead = tap_count - 1 - tap_index
        up_grad = up_grad + conv_weight[tap_index][None, :] * after[lead : lead + tok_rows]
    local_taps = jnp.stack(
        [
            jnp.sum(conv_grad * padded[tap_index : tap_index + tok_rows], axis=0)
            for tap_index in range(tap_count)
        ]
    )
    local_bias = jnp.sum(conv_grad, axis=0)
    partial_value = jnp.einsum("td,tf->df", full_cot, hidden, preferred_element_type=jnp.float32)
    weight_grad = summed_rows(partial_value, FS, 0)
    local_norms = jnp.sum(weight_grad * weight_grad, axis=0)
    tap_grad, bias_grad, unit_norms = (
        one_axis_at_a_time(local_taps, FS),
        one_axis_at_a_time(local_bias, FS),
        one_axis_at_a_time(local_norms, FS),
    )
    return (up_grad.astype(jnp.bfloat16), gate_grad, weight_grad, tap_grad, bias_grad, unit_norms)


def solution(mesh):
    finer = Mesh(mesh.devices.reshape(8, 8, mesh.shape["tp"]), ("fs_0", "fs_1", "tp"))
    return jax.shard_map(
        per_device,
        mesh=finer,
        in_specs=(P(FS, "tp"), P(FS, "tp"), P(FS, "tp"), P(FS, "tp"), P(None, "tp"), P("tp")),
        out_specs=(P(FS, "tp"), P(FS, "tp"), P(FS, "tp"), P(None, "tp"), P("tp"), P("tp")),
        check_vma=False,
    )
```

profile of v0, /device:TPU:4, one launch (start us, length us, event | category | flops | bytes accessed | tf_op | source)
XLA Modules:
  0.0 215.8 jit_solution(17460631630296203158)
XLA Ops:
  7.2 0.0 copy-start.1
  7.2 0.0 copy-start.2
  7.2 0.0 copy-start.5
  7.2 0.0 all-gather.2.cloned.1.call-start
  7.2 0.7 all-gather.2.cloned.1.call-update
  7.9 1.8 broadcast_in_dim.2
  9.8 23.4 %all-to-all-start = ((bf16[64,32,256]{2,1,0:T(8,128)(2,1)}), bf16[64,32,256]{2,1,0:T(8,128)(2,1)S(1)}, u32[]{:S(2)}, u32[]{:S(2)}) async-start(bf16[64,32,256]{2,1,0:T(8,128)(2,1)} %broadcast_in_dim.2), calls=%async_computation | async-start | bytes 2097152 | tf_op jit(solution)/shard_map/all_to_all | solution.py:24
  33.2 0.0 reduce-scatter.5.cloned.1.call-start
  33.2 0.0 copy-done.1
  33.2 3.5 %collective-permute-start = (bf16[2,256]{1,0:T(2,128)(2,1)S(1)}, bf16[2,256]{1,0:T(2,128)(2,1)S(1)}, u32[]{:S(2)}, u32[]{:S(2)}) collective-permute-start(bf16[2,256]{1,0:T(2,128)(2,1)S(1)} %slice.37), channel_id=1, source_target_pairs={{0,16},{16,32},{32,48},{48,64},{64,80},{80,96},{96,112},{112,128},... | collective-permute-start | bytes 3080 | tf_op jit(solution)/shard_map/ppermute | solution.py:13
  36.7 0.0 copy-done.2
  36.8 16.7 %collective-permute-done = bf16[2,256]{1,0:T(2,128)(2,1)S(1)} collective-permute-done((bf16[2,256]{1,0:T(2,128)(2,1)S(1)}, bf16[2,256]{1,0:T(2,128)(2,1)S(1)}, u32[]{:S(2)}, u32[]{:S(2)}) %collective-permute-start) | collective-permute-done | bytes 1056 | tf_op jit(solution)/shard_map/ppermute | solution.py:13
  53.5 0.1 maximum_convert_fusion
  53.6 9.4 %all-to-all-done = bf16[64,32,256]{2,1,0:T(8,128)(2,1)S(1)} async-done(((bf16[64,32,256]{2,1,0:T(8,128)(2,1)}), bf16[64,32,256]{2,1,0:T(8,128)(2,1)S(1)}, u32[]{:S(2)}, u32[]{:S(2)}) %all-to-all-start) | async-done | bytes 1048608 | tf_op jit(solution)/shard_map/all_to_all | solution.py:24
  63.0 8.3 %all-gather.2.cloned.1.call-done = bf16[768,2048]{1,0:T(8,128)(2,1)} async-done(((bf16[768,128]{1,0:T(8,128)(2,1)}), bf16[768,2048]{1,0:T(8,128)(2,1)}) %all-gather.2.cloned.1.call-update) | async-done | bytes 3145744 | tf_op jit(solution)/shard_map/all_gather | solution.py:60
  71.2 0.0 copy-done.5
  71.2 0.0 copy-start.3
  71.2 0.0 copy-start.4
  71.2 4.5 %multiply_reduce_fusion.2 = (f32[256]{0:T(256)S(1)}, f32[256]{0:T(256)S(1)}, f32[256]{0:T(256)S(1)}, f32[256]{0:T(256)S(1)}, f32[768,256]{1,0:T(8,128)S(1)}, /*index=5*/f32[768,256]{1,0:T(8,128)S(1)}, f32[768,256]{1,0:T(8,128)}) fusion(f32[770,256]{1,0:T(8,128)S(1)} %maximum_convert_fusion, bf16[768,256]{1,0:T(8,128)(2,1)} %param.7, f32[256]{0:T(256)S(1)} %bitcast.16, ...), kind=kOutput, calls=%fused_computation.17 | convolution fusion | flops 809827328 | bytes 9314304 | tf_op jit(solution)/shard_map/dot_general | solution.py:61
  75.7 0.0 copy-done.3
  75.7 0.0 copy-done.4
  75.7 2.5 %convolution_bitcast_fusion = f32[2048,256]{0,1:T(8,128)} fusion(bf16[768,2048]{1,0:T(8,128)(2,1)S(1)} %copy-done.3, bf16[768,256]{1,0:T(8,128)(2,1)S(1)} %copy-done.4, f32[768,256]{1,0:T(8,128)S(1)} %get-tuple-element.29), kind=kOutput, calls=%fused_computation | convolution fusion | flops 806682624 | bytes 6422528 | tf_op jit(solution)/shard_map/td,tf->df/dot_general | solution.py:79
  78.2 0.0 copy-start
  78.2 0.0 reduce-scatter.5.cloned.1.call-update
  78.2 0.0 reduce-scatter.7.cloned.1.call-start
  78.3 1.4 collective-permute-start.1
  79.7 48.7 %reduce-scatter.5.cloned.1.call-done = f32[256,256]{0,1:T(8,128)} async-done(((f32[2048,256]{0,1:T(8,128)}), f32[256,256]{0,1:T(8,128)}) %reduce-scatter.5.cloned.1.call-update) | async-done | bytes 262160 | tf_op jit(solution)/shard_map/reduce_scatter | solution.py:36
  128.4 1.8 copy.14
  130.2 0.0 reduce-scatter.7.cloned.1.call-update
  130.2 0.0 copy-done
  130.3 1.0 multiply_convert_fusion
  131.2 0.0 collective-permute-done.1
  131.3 1.0 fusion.4
  132.3 40.1 %reduce-scatter.7.cloned.1.call-done = f32[32,256]{1,0:T(8,128)} async-done(((f32[256,256]{1,0:T(8,128)}), f32[32,256]{1,0:T(8,128)}) %reduce-scatter.7.cloned.1.call-update) | async-done | bytes 32784
  172.3 0.9 copy.15
  173.2 0.1 multiply_reduce_fusion.3
  173.3 19.6 %all-reduce.1 = (f32[3,256]{1,0:T(4,128)S(1)}, f32[256]{0:T(256)S(1)}, f32[256]{0:T(256)S(1)}) all-reduce(f32[3,256]{1,0:T(4,128)S(1)} %pad_maximum_fusion.1, f32[256]{0:T(256)S(1)} %get-tuple-element.21, f32[256]{0:T(256)S(1)} %multiply_reduce_fusion.3), channel_id=1, replica_groups=mesh['fs_0'=8,'fs_1'=8,'tp'=16] {'fs_0'}, use_global_device_ids=true, to_apply=%region_5.0 | all-reduce | flops 1280 | bytes 10240 | tf_op jit(solution)/shard_map/psum | solution.py:42
  192.9 16.4 %all-reduce = (f32[3,256]{1,0:T(4,128)}, f32[256]{0:T(256)}, f32[256]{0:T(256)}) all-reduce(f32[3,256]{1,0:T(4,128)S(1)} %get-tuple-element.25, f32[256]{0:T(256)S(1)} %get-tuple-element.26, f32[256]{0:T(256)S(1)} %get-tuple-element.27), channel_id=1, replica_groups=mesh['fs_0'=8,'fs_1'=8,'tp'=16] {'fs_1'}, use_global_device_ids=true, to_apply=%region_6.0 | all-reduce | flops 1280 | bytes 10240 | tf_op jit(solution)/shard_map/psum | solution.py:42
  (4 shorter events, 0.0 us)
Async XLA Ops:
  7.2 26.1 %copy-start.1 = (bf16[768,256]{1,0:T(8,128)(2,1)S(1)}, bf16[768,256]{1,0:T(8,128)(2,1)}, u32[]{:S(2)}) copy-start(bf16[768,256]{1,0:T(8,128)(2,1)} %param.6) | copy-start | bytes 1179652
  7.2 29.6 %copy-start.2 = (f32[3,256]{1,0:T(4,128)S(1)}, f32[3,256]{1,0:T(4,128)}, u32[]{:S(2)}) copy-start(f32[3,256]{1,0:T(4,128)} %param.10) | copy-start | bytes 9220
  7.2 64.0 %copy-start.5 = (f32[256]{0:T(256)S(1)}, f32[256]{0:T(256)}, u32[]{:S(2)}) copy-start(f32[256]{0:T(256)} %param.11) | copy-start | bytes 3076
  7.2 64.0 %all-gather.2.cloned.1.call-start = ((), (), s32[]{:S(2)}) async-start(), calls=%async_computation.3 | async-start | bytes 3342336 | tf_op jit(solution)/shard_map/all_gather | solution.py:60
  9.8 53.2 %all-to-all-start = ((bf16[64,32,256]{2,1,0:T(8,128)(2,1)}), bf16[64,32,256]{2,1,0:T(8,128)(2,1)S(1)}, u32[]{:S(2)}, u32[]{:S(2)}) async-start(bf16[64,32,256]{2,1,0:T(8,128)(2,1)} %broadcast_in_dim.2), calls=%async_computation | async-start | bytes 2097152 | tf_op jit(solution)/shard_map/all_to_all | solution.py:24
  33.2 95.3 %reduce-scatter.5.cloned.1.call-start = ((), (), s32[]{:S(2)}) async-start(), calls=%async_computation.4 | async-start | bytes 2359296 | tf_op jit(solution)/shard_map/reduce_scatter | solution.py:36
  33.2 20.2 %collective-permute-start = (bf16[2,256]{1,0:T(2,128)(2,1)S(1)}, bf16[2,256]{1,0:T(2,128)(2,1)S(1)}, u32[]{:S(2)}, u32[]{:S(2)}) collective-permute-start(bf16[2,256]{1,0:T(2,128)(2,1)S(1)} %slice.37), channel_id=1, source_target_pairs={{0,16},{16,32},{32,48},{48,64},{64,80},{80,96},{96,112},{112,128},... | collective-permute-start | bytes 3080 | tf_op jit(solution)/shard_map/ppermute | solution.py:13
  71.2 4.5 %copy-start.3 = (bf16[768,2048]{1,0:T(8,128)(2,1)S(1)}, bf16[768,2048]{1,0:T(8,128)(2,1)}, u32[]{:S(2)}) copy-start(bf16[768,2048]{1,0:T(8,128)(2,1)} %all-gather.2.cloned.1.call-done) | copy-start | bytes 9437188
  71.2 4.5 %copy-start.4 = (bf16[768,256]{1,0:T(8,128)(2,1)S(1)}, bf16[768,256]{1,0:T(8,128)(2,1)}, u32[]{:S(2)}) copy-start(bf16[768,256]{1,0:T(8,128)(2,1)} %param.7) | copy-start | bytes 1179652
  78.2 52.1 %copy-start = (f32[768,256]{1,0:T(8,128)S(1)}, f32[768,256]{1,0:T(8,128)}, u32[]{:S(2)}) copy-start(f32[768,256]{1,0:T(8,128)} %get-tuple-element.33) | copy-start | bytes 2359300
  78.2 94.1 %reduce-scatter.7.cloned.1.call-start = ((), (), s32[]{:S(2)}) async-start(), calls=%async_computation.5 | async-start | bytes 294912
  78.3 53.0 %collective-permute-start.1 = (f32[2,256]{1,0:T(2,128)S(1)}, f32[2,256]{1,0:T(2,128)S(1)}, u32[]{:S(2)}, u32[]{:S(2)}) collective-permute-start(f32[2,256]{1,0:T(2,128)S(1)} %slice.49), channel_id=1, source_target_pairs={{16,0},{32,16},{48,32},{64,48},{80,64},{96,80},{112,96},{128,112},... | collective-permute-start | bytes 6152 | tf_op jit(solution)/shard_map/ppermute | solution.py:13
Sparse Core Ops, SparseCore 0:
  10.6 60.5 all-gather.1
  78.3 50.0 reduce-scatter.4
  132.4 39.8 reduce-scatter.6
where the time goes:
time: 216 us
  waiting for transfers between devices  124 us (57%)
  blocking collectives  36 us (17%)
  starting transfers between devices  28.4 us (13%)
  between operations  13.9 us (6%)
  matrix products  6.97 us (3%)
  local copies, waits for them, and re-layouts  4.5 us (2%)
  other arithmetic  2.18 us (1%)
    reduce_scatter x1, waiting for transfers between devices, summed_rows(): nearer = lax.psum_scatter(value, axes[0], scatter_dimension=dim, tiled=True)  48.7 us
    unnamed x4, waiting for transfers between devices  40.8 us
    psum x2, blocking collectives, one_axis_at_a_time(): value = lax.psum(value, axis)  36 us
    all_to_all x1, starting transfers between devices, from_everyone(): lax.all_to_all(jnp.broadcast_to(value[None], (peers, *value.shape)), axis...  23.4 us
    ppermute x2, waiting for transfers between devices, from_behind(): lax.ppermute(value, axis, [(source, source + steps) for source in range(i...  16.7 us
    all_to_all x1, waiting for transfers between devices, from_everyone(): lax.all_to_all(jnp.broadcast_to(value[None], (peers, *value.shape)), axis...  9.4 us
    all_gather x1, waiting for transfers between devices, per_device(): full_cot = lax.all_gather(out_cotangent, 'tp', axis=1, tiled=True)  8.26 us
    ppermute x2, starting transfers between devices, from_behind(): lax.ppermute(value, axis, [(source, source + steps) for source in range(i...  4.9 us
  transfers between devices with their start and end apart: 6, of which 5 were waited for; matrix products, arithmetic and copies ran while one was open for 3% of the time, Pallas kernels for 0%

commit v1 on v0

v1 whole, which is shorter than its diff:
```python
import functools

import jax
import jax.numpy as jnp
from jax import lax
from jax.experimental import pallas as pl
from jax.experimental.pallas import tpu as pltpu
from jax.sharding import PartitionSpec as P

MESH = pl.DeviceIdType.MESH
BF16 = jnp.bfloat16
F32 = jnp.float32


def ring_offsets(n):
    half = n // 2
    return [o for d in range(1, half + 1) for o in ((d, -d) if 2 * d < n else (d,))]


RELAY = {3: 2, 4: 2, -3: -2}


def kernel(dims, up, gate, cot, w, cw, cb, upg, gg, wg, tap, bias, nrm, *s):
    nx, ny, nz = dims
    (cot_all, wall, upf, act, dact, hid, hg, cgp, partf, partb, recv_a, send_b, recv_f,
     zsend, zrecv, zown, halo_up, halo_cg, ty, tz, qy, qz,
     x_s, x_r, sib_s, sib_r, wy_s, wy_r, wz_s, wz_r, a_s, a_r, f_s, f_r, z_s, z_r,
     h_s, h_r, ty_s, ty_r, tz_s, tz_r, qy_s, qy_r, qz_s, qz_r) = s
    tokens, width = up.shape
    half_t = tokens // 2
    tile = min(96, tokens // 2)
    hx, hz = nx // 2, nz // 2
    fs, tp = lax.axis_index("fs"), lax.axis_index("tp")
    x, c = lax.div(tp, 2), lax.rem(tp, 2)
    z, y = lax.div(fs, ny), lax.rem(fs, ny)

    def wrap(v, n):
        return lax.rem(v + 2 * n, n)

    def dev(x_=x, c_=c, y_=y, z_=z):
        return {"fs": z_ * ny + y_, "tp": x_ * 2 + c_}

    def flat(step):
        other = wrap(fs + step, ny * nz)
        return {"fs": other, "tp": tp}

    sends = []

    def rcopy(src, dst, ss, rs, to):
        return pltpu.make_async_remote_copy(
            src_ref=src, dst_ref=dst, send_sem=ss, recv_sem=rs, device_id=to, device_id_type=MESH
        )

    def send(src, dst, ss, rs, to):
        copy = rcopy(src, dst, ss, rs, to)
        copy.start()
        sends.append(copy)

    def arrived(dst, ss, rs, to):
        rcopy(dst, dst, ss, rs, to).wait_recv()

    sibling = dev(c_=1 - c)
    x_to = (dev(x_=wrap(x + 1, nx)), dev(x_=wrap(x - 1, nx)))
    z_to = (dev(z_=wrap(z + 1, nz)), dev(z_=wrap(z - 1, nz)))
    y_offs = ring_offsets(ny)
    relayed = [o for o in y_offs if o in RELAY]
    hubs = sorted({RELAY[o] for o in relayed})
    finals = [o for o in y_offs if o not in RELAY]

    barrier = pltpu.get_barrier_semaphore()
    peers = [sibling, *x_to, flat(1), flat(-1)]
    peers += [dev(y_=wrap(y + j, ny)) for j in range(1, ny)]
    peers += [dev(z_=wrap(z + j, nz)) for j in range(1, nz)]
    for peer in peers:
        pl.semaphore_signal(barrier, inc=1, device_id=peer, device_id_type=MESH)
    pl.semaphore_wait(barrier, len(peers))

    for h in range(2):
        for way in range(2):
            if hx == 1 and h != way:
                continue
            send(cot.at[pl.ds(h * half_t, half_t)], cot_all.at[x, c, h],
                 x_s.at[way, 0, h], x_r.at[way, 0, h], x_to[way])
    send(up.at[pl.ds(tokens - 16, 16)], halo_up, h_s.at[0], h_r.at[0], flat(1))
    for j in range(1, ny):
        send(w, wall.at[z, y], wy_s.at[j - 1], wy_r.at[j - 1], dev(y_=wrap(y + j, ny)))
    for h in range(2):
        send(cot.at[pl.ds(h * half_t, half_t)], cot_all.at[x, c, h],
             sib_s.at[0, 0, h], sib_r.at[0, 0, h], sibling)
    wall[z, y] = w[...]
    for h in range(2):
        cot_all[x, c, h] = cot[pl.ds(h * half_t, half_t), :]

    taps = [cw[pl.ds(k, 1), :] for k in range(3)]
    bias_row = cb[...]

    def widen(i, carry):
        base = pl.multiple_of(i * tile, 16)
        upf[pl.ds(base + 8, tile), :] = up[pl.ds(base, tile), :].astype(F32)
        return carry

    lax.fori_loop(0, tokens // tile, widen, 0)

    def shifted_up(base):
        rows = upf[pl.ds(base, tile + 8), :]
        return [rows[6 + k : 6 + k + tile] for k in range(3)]

    def forward(i, carry):
        base = pl.multiple_of(i * tile, 16)
        conv = bias_row
        for k, rows in enumerate(shifted_up(base)):
            conv = conv + taps[k] * rows
        sig = 1.0 / (1.0 + jnp.exp(-conv))
        gate_f = gate[pl.ds(base, tile), :].astype(F32)
        activated = conv * sig
        act[pl.ds(base, tile), :] = activated
        dact[pl.ds(base, tile), :] = gate_f * sig * (1.0 + conv * (1.0 - sig))
        hid[pl.ds(base, tile), :] = (activated * gate_f).astype(BF16)
        return carry

    lax.fori_loop(1, tokens // tile, forward, 0)
    arrived(halo_up, h_s.at[0], h_r.at[0], flat(1))
    upf[0:8, :] = jnp.where(fs > 0, halo_up[...].astype(F32)[8:16], 0.0)
    forward(0, 0)

    for j in range(1, ny):
        arrived(wall.at[z, wrap(y - j, ny)], wy_s.at[j - 1], wy_r.at[j - 1], sibling)
    half_y = ny // 2

    def w_piece(z_, h):
        return wall.at[z_, pl.ds(h * half_y, half_y)]

    def w_send(way, step, h):
        if step >= hz or (step == hz - 1 and h != way):
            return
        piece = w_piece(wrap(z - step if way == 0 else z + step, nz), h)
        send(piece, piece, wz_s.at[way, step, h], wz_r.at[way, step, h], z_to[way])

    def w_arrive(way, d, h):
        if d == hz and h != way:
            return
        piece = w_piece(wrap(z - d if way == 0 else z + d, nz), h)
        arrived(piece, wz_s.at[way, d - 1, h], wz_r.at[way, d - 1, h], z_to[way])
        w_send(way, d, h)

    for h in range(2):
        for way in range(2):
            w_send(way, 0, h)

    def origin(k):
        d = (k + 1) // 2
        return wrap(x - d if (k % 2 == 1 or d == hx) else x + d, nx)

    def wgrad(k):
        org = origin(k)
        for cc in range(2):
            block = cot_all[org, cc].reshape(tokens, cot.shape[1])
            part = lax.dot_general(block, hid[...], (((0,), (0,)), ((), ())),
                                   preferred_element_type=F32)
            part = part.reshape(half_y, w.shape[0], width)
            partf[k, pl.ds(cc * half_y, half_y)] = part
            partb[k, pl.ds(cc * half_y, half_y)] = part.astype(BF16)

    def rs_first(k):
        for o in y_offs:
            target = wrap(y - o, ny)
            if o in RELAY:
                i = relayed.index(o)
                send(partb.at[k, target], recv_a.at[k, i], a_s.at[k, i], a_r.at[k, i],
                     dev(y_=wrap(y - o + RELAY[o], ny)))
            elif o not in hubs:
                i = finals.index(o)
                send(partb.at[k, target], recv_f.at[k, i], f_s.at[k, i], f_r.at[k, i],
                     dev(y_=target))

    def rs_second(k):
        for b, r in enumerate(hubs):
            target = wrap(y - r, ny)
            total = partf[k, target]
            for i, o in enumerate(relayed):
                if RELAY[o] == r:
                    arrived(recv_a.at[k, i], a_s.at[k, i], a_r.at[k, i], sibling)
                    total = total + recv_a[k, i].astype(F32)
            send_b[k, b] = total.astype(BF16)
            i = finals.index(r)
            send(send_b.at[k, b], recv_f.at[k, i], f_s.at[k, i], f_r.at[k, i], dev(y_=target))

    def z_copy(k):
        org = origin(k)
        slot = wrap(z - org - 1, nz)
        return rcopy(zsend.at[k], zrecv.at[slot], z_s.at[k], z_r.at[slot], dev(z_=org))

    def rs_third(k):
        total = partf[k, y]
        for i in range(len(finals)):
            arrived(recv_f.at[k, i], f_s.at[k, i], f_r.at[k, i], sibling)
            total = total + recv_f[k, i].astype(F32)

        @pl.when(origin(k) == z)
        def _():
            zown[...] = total

        @pl.when(origin(k) != z)
        def _():
            zsend[k] = total.astype(BF16)
            z_copy(k).start()

    def chunks(d):
        return [k for k in range(nx) if (k + 1) // 2 == d]

    for h in range(2):
        arrived(cot_all.at[x, 1 - c, h], sib_s.at[0, 0, h], sib_r.at[0, 0, h], sibling)
    wgrad(0)
    rs_first(0)

    def grad_hidden(j, carry):
        org = wrap(x - hx + 1 + j, nx)
        weights = wall[org].reshape(ny * w.shape[0], width)
        for h in range(2):
            rows = jnp.concatenate([cot_all[org, 0, h], cot_all[org, 1, h]], axis=-1)
            hg[h] += jnp.dot(rows, weights, preferred_element_type=F32)
        return carry

    hg[...] = jnp.zeros_like(hg)

    for d in range(1, hx + 1):
        if d == hx:
            for dd in range(d, hz + 1):
                for h in range(2):
                    for way in range(2):
                        w_arrive(way, dd, h)
            lax.fori_loop(0, nx - 1, grad_hidden, 0)
        for h in range(2):
            for way in range(2):
                if d == hx and h != way:
                    continue
                org = wrap(x - d if way == 0 else x + d, nx)
                piece = cot_all.at[org, c, h]
                arrived(piece, x_s.at[way, d - 1, h], x_r.at[way, d - 1, h], x_to[way])
                if d < hx and not (d == hx - 1 and h != way):
                    send(piece, piece, x_s.at[way, d, h], x_r.at[way, d, h], x_to[way])
                send(piece, piece, sib_s.at[way, d, h], sib_r.at[way, d, h], sibling)
            if d < hx:
                for way in range(2):
                    w_arrive(way, d, h)
        for k in chunks(d - 1):
            rs_second(k)
        if d >= 2:
            for k in chunks(d - 2):
                rs_third(k)
        for h in range(2):
            for way in range(2):
                if d == hx and h != way:
                    continue
                org = wrap(x - d if way == 0 else x + d, nx)
                arrived(cot_all.at[org, 1 - c, h], sib_s.at[way, d, h], sib_r.at[way, d, h], sibling)
        for k in chunks(d):
            wgrad(k)
            rs_first(k)

    grad_hidden(nx - 1, 0)
    rows_h = half_t // tile

    def eight(v):
        return jnp.sum(v.reshape(tile // 8, 8, width), axis=0)

    def backward(i, sums):
        base = pl.multiple_of(i * tile, 16)
        grad = hg[lax.div(i, rows_h), pl.ds(pl.multiple_of(lax.rem(i, rows_h) * tile, 16), tile), :]
        gg[pl.ds(base, tile), :] = (grad * act[pl.ds(base, tile), :]).astype(BF16)
        conv_grad = grad * dact[pl.ds(base, tile), :]
        cgp[pl.ds(base, tile), :] = conv_grad
        ups = shifted_up(base)
        return tuple(sums[k] + eight(conv_grad * ups[k]) for k in range(3)) + (
            sums[3] + eight(conv_grad),
        )

    zero = jnp.zeros((8, width), F32)
    sums = backward(0, (zero,) * 4)
    send(cgp.at[pl.ds(0, 8)], halo_cg, h_s.at[1], h_r.at[1], flat(-1))
    sums = lax.fori_loop(1, tokens // tile, backward, sums)
    for k in chunks(hx - 1):
        rs_third(k)
    for k in chunks(hx):
        rs_second(k)
    row = jnp.concatenate([jnp.sum(v, axis=0, keepdims=True) for v in sums], axis=0)
    ty[y] = row
    for j in range(1, ny):
        send(ty.at[y], ty.at[y], ty_s.at[j - 1], ty_r.at[j - 1], dev(y_=wrap(y + j, ny)))

    def up_grads(i, carry):
        base = pl.multiple_of(i * tile, 16)
        rows = cgp[pl.ds(base, tile + 8), :]
        total = taps[0] * rows[2 : 2 + tile] + taps[1] * rows[1 : 1 + tile] + taps[2] * rows[0:tile]
        upg[pl.ds(base, tile), :] = total.astype(BF16)
        return carry

    lax.fori_loop(0, tokens // tile - 1, up_grads, 0)
    for k in chunks(hx):
        rs_third(k)
    arrived(halo_cg, h_s.at[1], h_r.at[1], flat(-1))
    cgp[pl.ds(tokens, 8), :] = jnp.where(fs < ny * nz - 1, halo_cg[...], 0.0)
    up_grads(tokens // tile - 1, 0)

    def gather(buf, n, me, ss, rs, first):
        if first:
            for j in range(1, n):
                to = dev(y_=wrap(y + j, ny)) if buf is ty or buf is qy else dev(z_=wrap(z + j, nz))
                send(buf.at[me], buf.at[me], ss.at[j - 1], rs.at[j - 1], to)
            return None
        for j in range(1, n):
            arrived(buf.at[wrap(me - j, n)], ss.at[j - 1], rs.at[j - 1], sibling)
        total = buf[0]
        for j in range(1, n):
            total = total + buf[j]
        return total

    tz[z] = gather(ty, ny, y, ty_s, ty_r, False)
    gather(tz, nz, z, tz_s, tz_r, True)

    total = zown[...]
    for j in range(nz - 1):
        arrived(zrecv.at[j], z_s.at[0], z_r.at[j], sibling)
    for j in range(nz - 1):
        total = total + zrecv[j].astype(F32)
    wg[...] = total
    qy[y] = jnp.sum(total * total, axis=0, keepdims=True)
    gather(qy, ny, y, qy_s, qy_r, True)
    taps_total = gather(tz, nz, z, tz_s, tz_r, False)
    tap[...] = taps_total[0:3]
    bias[...] = taps_total[3:4]
    qz[z] = gather(qy, ny, y, qy_s, qy_r, False)
    gather(qz, nz, z, qz_s, qz_r, True)
    nrm[...] = gather(qz, nz, z, qz_s, qz_r, False)

    for copy in sends:
        copy.wait_send()
    for k in range(nx):

        @pl.when(origin(k) != z)
        def _(k=k):
            z_copy(k).wait_send()


def per_device(dims, up_pre, gate_value, out_cotangent, down_weight, conv_weight, conv_bias):
    nx, ny, nz = dims
    tokens, width = up_pre.shape
    depth, rows = out_cotangent.shape[1], down_weight.shape[0]
    hx, hz = nx // 2, nz // 2
    y_offs = ring_offsets(ny)
    n_rel = max(1, len([o for o in y_offs if o in RELAY]))
    n_fin = len([o for o in y_offs if o not in RELAY])
    vmem, dma = pltpu.VMEM, pltpu.SemaphoreType.DMA
    scratch = [
        vmem((nx, 2, 2, tokens // 2, depth), BF16),
        vmem((nz, ny, rows, width), BF16),
        vmem((tokens + 8, width), F32),
        vmem((tokens, width), F32),
        vmem((tokens, width), F32),
        vmem((tokens, width), BF16),
        vmem((2, tokens // 2, width), F32),
        vmem((tokens + 8, width), F32),
        vmem((nx, ny, rows, width), F32),
        vmem((nx, ny, rows, width), BF16),
        vmem((nx, n_rel, rows, width), BF16),
        vmem((nx, 2, rows, width), BF16),
        vmem((nx, n_fin, rows, width), BF16),
        vmem((nx, rows, width), BF16),
        vmem((nz - 1, rows, width), BF16),
        vmem((rows, width), F32),
        vmem((16, width), BF16),
        vmem((8, width), F32),
        vmem((ny, 4, width), F32),
        vmem((nz, 4, width), F32),
        vmem((ny, 1, width), F32),
        vmem((nz, 1, width), F32),
        dma((2, hx, 2)), dma((2, hx, 2)),
        dma((2, hx + 1, 2)), dma((2, hx + 1, 2)),
        dma((ny - 1,)), dma((ny - 1,)),
        dma((2, hz, 2)), dma((2, hz, 2)),
        dma((nx, n_rel)), dma((nx, n_rel)),
        dma((nx, n_fin)), dma((nx, n_fin)),
        dma((nx,)), dma((nz - 1,)),
        dma((2,)), dma((2,)),
        dma((ny - 1,)), dma((ny - 1,)),
        dma((nz - 1,)), dma((nz - 1,)),
        dma((ny - 1,)), dma((ny - 1,)),
        dma((nz - 1,)), dma((nz - 1,)),
    ]
    spec = pl.BlockSpec(memory_space=pltpu.VMEM)
    up_grad, gate_grad, weight_grad, tap_grad, bias_grad, unit_norms = pl.pallas_call(
        functools.partial(kernel, dims),
        out_shape=(
            jax.ShapeDtypeStruct((tokens, width), BF16),
            jax.ShapeDtypeStruct((tokens, width), BF16),
            jax.ShapeDtypeStruct((rows, width), F32),
            jax.ShapeDtypeStruct((3, width), F32),
            jax.ShapeDtypeStruct((1, width), F32),
            jax.ShapeDtypeStruct((1, width), F32),
        ),
        in_specs=[spec] * 6,
        out_specs=(spec,) * 6,
        scratch_shapes=scratch,
        compiler_params=pltpu.CompilerParams(
            collective_id=0, has_side_effects=True, vmem_limit_bytes=40 * 1024 * 1024
        ),
    )(up_pre, gate_value, out_cotangent, down_weight, conv_weight, conv_bias[None])
    return up_grad, gate_grad, weight_grad, tap_grad, bias_grad[0], unit_norms[0]


def solution(mesh):
    nx = mesh.shape["tp"] // 2
    dims = (nx, mesh.shape["fs"] // nx, nx)
    return jax.shard_map(
        functools.partial(per_device, dims),
        mesh=mesh,
        in_specs=(P("fs", "tp"), P("fs", "tp"), P("fs", "tp"), P("fs", "tp"), P(None, "tp"), P("tp")),
        out_specs=(P("fs", "tp"), P("fs", "tp"), P("fs", "tp"), P(None, "tp"), P("tp"), P("tp")),
        check_vma=False,
    )
```

time: 216 us -> 84.5 us (0.39)
  the two profiles are of different devices: /device:TPU:4 before, /device:TPU:2 now
where the time goes in v1:
time: 84.5 us; the launch traced here: 84.2 us
  Pallas kernels  74.7 us (88%)
  local copies, waits for them, and re-layouts  8.82 us (10%)
    pallas_call x1, Pallas kernels, per_device(): pl.pallas_call(functools.partial(kernel, dims), out_shape=(jax.ShapeDtype...  74.7 us
    unnamed x18, local copies, waits for them, and re-layouts  8.82 us

profile of v1, /device:TPU:2, one launch (start us, length us, event | category | flops | bytes accessed | tf_op | source)
XLA Modules:
  0.0 84.2 jit_solution(12474681189937749351)
XLA Ops:
  0.6 0.0 copy-start.5
  0.6 0.7 copy-done.5
  1.3 0.0 copy-start
  1.3 1.0 %copy-done = bf16[768,256]{1,0:T(8,128)(2,1)S(1)} copy-done((bf16[768,256]{1,0:T(8,128)(2,1)S(1)}, bf16[768,256]{1,0:T(8,128)(2,1)}, u32[]{:S(2)}) %copy-start) | copy-done | bytes 393240
  2.3 0.0 copy-start.1
  2.3 1.0 %copy-done.1 = bf16[768,256]{1,0:T(8,128)(2,1)S(1)} copy-done((bf16[768,256]{1,0:T(8,128)(2,1)S(1)}, bf16[768,256]{1,0:T(8,128)(2,1)}, u32[]{:S(2)}) %copy-start.1) | copy-done | bytes 393240
  3.3 0.0 copy-start.2
  3.3 0.9 %copy-done.2 = bf16[768,128]{1,0:T(8,128)(2,1)S(1)} copy-done((bf16[768,128]{1,0:T(8,128)(2,1)S(1)}, bf16[768,128]{1,0:T(8,128)(2,1)}, u32[]{:S(2)}) %copy-start.2) | copy-done | bytes 196632
  4.2 0.0 copy-start.3
  4.2 0.7 copy-done.3
  5.0 0.0 copy-start.4
  5.0 0.7 copy-done.4
  5.6 74.7 %shard_map.109 = (bf16[768,256]{1,0:T(8,128)(2,1)S(1)}, bf16[768,256]{1,0:T(8,128)(2,1)S(1)}, f32[32,256]{1,0:T(8,128)S(1)}, f32[3,256]{1,0:T(4,128)S(1)}, f32[1,256]{1,0:T(1,128)S(1)}, /*index=5*/f32[1,256]{1,0:T(1,128)S(1)}) custom-call(bf16[768,256]{1,0:T(8,128)(2,1)S(1)} %copy-done, bf16[768,256]{1,0:T(8,128)(2,1)S(1)} %copy-done.1, ...), custom_call_target="tpu_custom_call" | custom-call | tf_op jit(solution)/shard_map/pallas_call | solution.py:391
  80.4 0.7 copy.18
  81.1 0.7 copy.19
  81.9 0.6 copy.20
  82.5 0.6 copy.21
  83.1 0.6 copy.22
  83.6 0.6 copy.23
Async XLA Ops:
  0.6 0.7 copy-start.5
  1.3 1.0 %copy-start = (bf16[768,256]{1,0:T(8,128)(2,1)S(1)}, bf16[768,256]{1,0:T(8,128)(2,1)}, u32[]{:S(2)}) copy-start(bf16[768,256]{1,0:T(8,128)(2,1)} %up.1) | copy-start | bytes 1179652
  2.3 1.0 %copy-start.1 = (bf16[768,256]{1,0:T(8,128)(2,1)S(1)}, bf16[768,256]{1,0:T(8,128)(2,1)}, u32[]{:S(2)}) copy-start(bf16[768,256]{1,0:T(8,128)(2,1)} %gate.1) | copy-start | bytes 1179652
  3.3 0.9 %copy-start.2 = (bf16[768,128]{1,0:T(8,128)(2,1)S(1)}, bf16[768,128]{1,0:T(8,128)(2,1)}, u32[]{:S(2)}) copy-start(bf16[768,128]{1,0:T(8,128)(2,1)} %cot.1) | copy-start | bytes 589828
  4.2 0.7 copy-start.3
  5.0 0.7 copy-start.4

commit v2 on v1

v2 whole, which is shorter than its diff:
```python
import functools

import jax
import jax.numpy as jnp
from jax import lax
from jax.experimental import pallas as pl
from jax.experimental.pallas import tpu as pltpu
from jax.sharding import PartitionSpec as P

MESH = pl.DeviceIdType.MESH
BF16 = jnp.bfloat16
F32 = jnp.float32


def ring_offsets(n):
    half = n // 2
    return [o for d in range(1, half + 1) for o in ((d, -d) if 2 * d < n else (d,))]


RELAY = {3: 2, 4: 2, -3: -2}


def kernel(dims, up_in, gate_in, cot_in, w_in, cw_in, cb_in, upg, gg, wg, tap, bias, nrm, *s):
    nx, ny, nz = dims
    (cot_all, wall, upf, act, dact, hid, hg, cgp, partf, partb, recv_a, send_b, recv_f,
     zsend, zrecv, zown, halo_up, halo_cg, ty, tz, qy, qz, up, gate, cw, cb,
     in_s, x_s, x_r, sib_s, sib_r, wy_s, wy_r, wz_s, wz_r, a_s, a_r, f_s, f_r, z_s, z_r,
     h_s, h_r, sum_s, sum_r) = s
    tokens, width = up_in.shape
    depth, n_rows = cot_in.shape[1], w_in.shape[0]
    half_t, half_y = tokens // 2, ny // 2
    tile = min(96, tokens // 2)
    tiles = tokens // tile
    hx, hz = nx // 2, nz // 2
    fs, tp = lax.axis_index("fs"), lax.axis_index("tp")
    x, c = lax.div(tp, 2), lax.rem(tp, 2)
    z, y = lax.div(fs, ny), lax.rem(fs, ny)

    def wrap(v, n):
        return lax.rem(v + 2 * n, n)

    def dev(x_=x, c_=c, y_=y, z_=z):
        return {"fs": z_ * ny + y_, "tp": x_ * 2 + c_}

    def flat(step):
        return {"fs": wrap(fs + step, ny * nz), "tp": tp}

    sibling = dev(c_=1 - c)
    x_to = (dev(x_=wrap(x + 1, nx)), dev(x_=wrap(x - 1, nx)))
    z_to = (dev(z_=wrap(z + 1, nz)), dev(z_=wrap(z - 1, nz)))

    def rcopy(src, dst, ss, rs, to):
        return pltpu.make_async_remote_copy(
            src_ref=src, dst_ref=dst, send_sem=ss, recv_sem=rs, device_id=to, device_id_type=MESH
        )

    def send(src, dst, ss, rs, to):
        rcopy(src, dst, ss, rs, to).start()

    def arrived(size_of, rs):
        rcopy(size_of, size_of, x_s.at[0], rs, sibling).wait_recv()

    def sent(size_of, ss):
        rcopy(size_of, size_of, ss, z_r.at[0], sibling).wait_send()

    def load(src, dst, i):
        copy = pltpu.make_async_copy(src, dst, in_s.at[i])
        copy.start()
        return copy

    cot_loads = [
        load(cot_in.at[pl.ds(h * half_t, half_t)], cot_all.at[x, c, h], h) for h in range(2)
    ]
    w_load = load(w_in, wall.at[z, y], 2)
    up_load = load(up_in, up, 3)
    gate_load = load(gate_in, gate, 4)
    row_loads = [load(cw_in, cw, 5), load(cb_in, cb, 6)]

    barrier = pltpu.get_barrier_semaphore()
    peers = [sibling, *x_to, flat(1), flat(-1)]
    peers += [dev(y_=wrap(y + j, ny)) for j in range(1, ny)]
    peers += [dev(z_=wrap(z + j, nz)) for j in range(1, nz)]
    for peer in peers:
        pl.semaphore_signal(barrier, inc=1, device_id=peer, device_id_type=MESH)
    pl.semaphore_wait(barrier, len(peers))

    w_load.wait()
    for j in range(1, ny):
        send(wall.at[z, y], wall.at[z, y], wy_s.at[0], wy_r.at[0], dev(y_=wrap(y + j, ny)))

    def x_piece(way, d, j):
        return wrap(x - d if way == 0 else x + d, nx), (j if way == 0 else 1 - j)

    def x_send(way, d, j):
        if d < hx and not (d == hx - 1 and j == 1):
            org, h = x_piece(way, d, j)
            piece = cot_all.at[org, c, h]
            send(piece, piece, x_s.at[0], x_r.at[way, d, j], x_to[way])

    def x_step(d, j):
        for way in range(2):
            org, h = x_piece(way, d, j)
            piece = cot_all.at[org, c, h]
            arrived(piece, x_r.at[way, d - 1, j])
            x_send(way, d, j)
            send(piece, piece, sib_s.at[0], sib_r.at[d], sibling)

    for copy in cot_loads:
        copy.wait()
    for j in range(2):
        for way in range(2):
            x_send(way, 0, j)
    for h in range(2):
        send(cot_all.at[x, c, h], cot_all.at[x, c, h], sib_s.at[0], sib_r.at[0], sibling)
    up_load.wait()
    send(up.at[pl.ds(tokens - 16, 16)], halo_up, h_s.at[0], h_r.at[0], flat(1))
    gate_load.wait()
    for copy in row_loads:
        copy.wait()

    taps = [cw[pl.ds(k, 1), :] for k in range(3)]
    bias_row = cb[...]

    def widen(i, carry):
        base = pl.multiple_of(i * tile, 16)
        upf[pl.ds(base + 8, tile), :] = up[pl.ds(base, tile), :].astype(F32)
        return carry

    lax.fori_loop(0, tiles, widen, 0)

    def shifted_up(base):
        rows = upf[pl.ds(base, tile + 8), :]
        return [rows[6 + k : 6 + k + tile] for k in range(3)]

    def forward(i, carry):
        base = pl.multiple_of(i * tile, 16)
        conv = bias_row
        for k, rows in enumerate(shifted_up(base)):
            conv = conv + taps[k] * rows
        sig = 1.0 / (1.0 + jnp.exp(-conv))
        gate_f = gate[pl.ds(base, tile), :].astype(F32)
        activated = conv * sig
        act[pl.ds(base, tile), :] = activated
        dact[pl.ds(base, tile), :] = gate_f * sig * (1.0 + conv * (1.0 - sig))
        hid[pl.ds(base, tile), :] = (activated * gate_f).astype(BF16)
        return carry

    lax.fori_loop(1, tiles, forward, 0)
    arrived(halo_up, h_r.at[0])
    upf[0:8, :] = jnp.where(fs > 0, halo_up[...].astype(F32)[8:16], 0.0)
    forward(0, 0)

    def w_piece(way, d, j):
        h = j if way == 0 else 1 - j
        return wall.at[wrap(z - d if way == 0 else z + d, nz), pl.ds(h * half_y, half_y)]

    def w_send(way, d, j):
        if d < hz and not (d == hz - 1 and j == 1):
            piece = w_piece(way, d, j)
            send(piece, piece, wz_s.at[0], wz_r.at[way, d, j], z_to[way])

    w_left = [(d, j) for d in range(1, hz + 1) for j in range(2) if not (d == hz and j == 1)]

    def w_steps(count):
        for _ in range(min(count, len(w_left))):
            d, j = w_left.pop(0)
            for way in range(2):
                arrived(w_piece(way, d, j), wz_r.at[way, d - 1, j])
                w_send(way, d, j)

    def origin(k):
        d = (k + 1) // 2
        return wrap(x - d if (k % 2 == 1 or d == hx) else x + d, nx)

    def wgrad(k, cc):
        block = cot_all[origin(k), cc].reshape(tokens, depth)
        part = lax.dot_general(block, hid[...], (((0,), (0,)), ((), ())),
                               preferred_element_type=F32)
        part = part.reshape(half_y, n_rows, width)
        partf[k, pl.ds(cc * half_y, half_y)] = part
        partb[k, pl.ds(cc * half_y, half_y)] = part.astype(BF16)

    offsets = ring_offsets(ny)
    relayed = [o for o in offsets if o in RELAY]
    hubs = sorted({RELAY[o] for o in relayed})
    finals = [o for o in offsets if o not in RELAY]

    def turned(k, o):
        return o if k % 2 == 0 else -o

    def rs_first(k):
        for o in relayed:
            target, via = wrap(y - turned(k, o), ny), wrap(y - turned(k, o - RELAY[o]), ny)
            send(partb.at[k, target], recv_a.at[k, relayed.index(o)], a_s.at[0], a_r.at[k],
                 dev(y_=via))
        for i, o in enumerate(finals):
            if o not in hubs:
                target = wrap(y - turned(k, o), ny)
                send(partb.at[k, target], recv_f.at[k, i], f_s.at[0], f_r.at[k], dev(y_=target))

    def rs_second(k):
        if relayed:
            arrived(recv_a.at[k], a_r.at[k])
        for b, r in enumerate(hubs):
            target = wrap(y - turned(k, r), ny)
            total = partf[k, target]
            for i, o in enumerate(relayed):
                if RELAY[o] == r:
                    total = total + recv_a[k, i].astype(F32)
            send_b[k, b] = total.astype(BF16)
            send(send_b.at[k, b], recv_f.at[k, finals.index(r)], f_s.at[0], f_r.at[k],
                 dev(y_=target))

    def rs_third(k):
        org = origin(k)
        arrived(recv_f.at[k], f_r.at[k])
        total = partf[k, y]
        for i in range(len(finals)):
            total = total + recv_f[k, i].astype(F32)

        @pl.when(org == z)
        def _():
            zown[...] = total

        @pl.when(org != z)
        def _():
            zsend[k] = total.astype(BF16)
            send(zsend.at[k], zrecv.at[wrap(z - org - 1, nz)], z_s.at[0], z_r.at[0], dev(z_=org))

    def chunks(d):
        return [k for k in range(nx) if (k + 1) // 2 == d]

    left = {"second": 0, "third": 0}

    def reduce_steps(second, third):
        while left["second"] <= min(second, hx):
            for k in chunks(left["second"]):
                rs_second(k)
            left["second"] += 1
        while left["third"] <= min(third, hx):
            for k in chunks(left["third"]):
                rs_third(k)
            left["third"] += 1

    def own_chunks(d):
        for k in chunks(d):
            wgrad(k, c)
        arrived(cot_all.at[pl.ds(0, len(chunks(d))), 0], sib_r.at[d])
        for k in chunks(d):
            wgrad(k, 1 - c)
            rs_first(k)

    x_step(1, 0)
    arrived(wall.at[z, pl.ds(0, ny - 1)], wy_r.at[0])
    for j in range(2):
        for way in range(2):
            w_send(way, 0, j)
    own_chunks(0)
    for d in range(1, hx):
        x_step(d, 1)
        if d >= 2:
            w_steps(1)
            reduce_steps(d - 2, d - 3)
        if d < hx - 1:
            x_step(d + 1, 0)
        own_chunks(d)
        if d < hx - 1:
            w_steps(1)
    if hx > 1:
        x_step(hx, 0)
    own_chunks(hx)

    w_steps(1)
    reduce_steps(hx - 2, hx - 3)
    w_steps(1)

    hg[...] = jnp.zeros_like(hg)

    def grad_hidden(org, carry):
        weights = wall[org].reshape(ny * n_rows, width)
        for h in range(2):
            rows = jnp.concatenate([cot_all[org, 0, h], cot_all[org, 1, h]], axis=-1)
            hg[h] += jnp.dot(rows, weights, preferred_element_type=F32)
        return carry

    def grad_hidden_near(e, carry):
        return grad_hidden(wrap(z - hz + 1 + e, nz), carry)

    lax.fori_loop(0, nz - 1, grad_hidden_near, 0)
    reduce_steps(hx - 1, hx - 2)
    reduce_steps(hx, hx - 2)
    w_steps(len(w_left))
    grad_hidden(wrap(z + hz, nz), 0)
    rows_h = half_t // tile

    def eight(v):
        return jnp.sum(v.reshape(tile // 8, 8, width), axis=0)

    def backward(i, sums):
        base = pl.multiple_of(i * tile, 16)
        grad = hg[lax.div(i, rows_h), pl.ds(pl.multiple_of(lax.rem(i, rows_h) * tile, 16), tile), :]
        gg[pl.ds(base, tile), :] = (grad * act[pl.ds(base, tile), :]).astype(BF16)
        conv_grad = grad * dact[pl.ds(base, tile), :]
        cgp[pl.ds(base, tile), :] = conv_grad
        ups = shifted_up(base)
        return tuple(sums[k] + eight(conv_grad * ups[k]) for k in range(3)) + (
            sums[3] + eight(conv_grad),
        )

    zero = jnp.zeros((8, width), F32)
    sums = backward(0, (zero,) * 4)
    send(cgp.at[pl.ds(0, 8)], halo_cg, h_s.at[1], h_r.at[1], flat(-1))
    reduce_steps(hx, hx - 1)
    sums = lax.fori_loop(1, tiles, backward, sums)
    row = jnp.concatenate([jnp.sum(v, axis=0, keepdims=True) for v in sums], axis=0)

    sum_bufs = (ty, tz, qy, qz)

    def share(i, value):
        buf, n, me = sum_bufs[i], (ny, nz)[i % 2], (y, z)[i % 2]
        buf[me] = value
        for j in range(1, n):
            to = dev(y_=wrap(y + j, ny)) if i % 2 == 0 else dev(z_=wrap(z + j, nz))
            send(buf.at[me], buf.at[me], sum_s.at[i], sum_r.at[i], to)

    def shared_total(i):
        buf, n = sum_bufs[i], (ny, nz)[i % 2]
        arrived(buf.at[pl.ds(0, n - 1)], sum_r.at[i])
        total = buf[0]
        for j in range(1, n):
            total = total + buf[j]
        return total

    share(0, row)
    reduce_steps(hx, hx)

    def up_grads(i, carry):
        base = pl.multiple_of(i * tile, 16)
        rows = cgp[pl.ds(base, tile + 8), :]
        total = taps[0] * rows[2 : 2 + tile] + taps[1] * rows[1 : 1 + tile] + taps[2] * rows[0:tile]
        upg[pl.ds(base, tile), :] = total.astype(BF16)
        return carry

    lax.fori_loop(0, tiles - 1, up_grads, 0)
    arrived(halo_cg, h_r.at[1])
    cgp[pl.ds(tokens, 8), :] = jnp.where(fs < ny * nz - 1, halo_cg[...], 0.0)
    up_grads(tiles - 1, 0)
    share(1, shared_total(0))

    arrived(zrecv, z_r.at[0])
    total = zown[...]
    for j in range(nz - 1):
        total = total + zrecv[j].astype(F32)
    wg[...] = total
    share(2, jnp.sum(total * total, axis=0, keepdims=True))
    taps_total = shared_total(1)
    tap[...] = taps_total[0:3]
    bias[...] = taps_total[3:4]
    share(3, shared_total(2))
    sent(cot_all.at[pl.ds(0, nx - 1), 0], x_s.at[0])
    sent(cot_all.at[:, 0], sib_s.at[0])
    sent(wall.at[0, pl.ds(0, ny - 1)], wy_s.at[0])
    sent(wall.at[pl.ds(0, nz - 1)], wz_s.at[0])
    if relayed:
        sent(recv_a, a_s.at[0])
    sent(recv_f, f_s.at[0])
    sent(zrecv, z_s.at[0])
    sent(halo_up, h_s.at[0])
    sent(halo_cg, h_s.at[1])
    for i in range(3):
        sent(sum_bufs[i].at[pl.ds(0, (ny, nz)[i % 2] - 1)], sum_s.at[i])
    nrm[...] = shared_total(3)
    sent(qz.at[pl.ds(0, nz - 1)], sum_s.at[3])


def store(*refs):
    sources, targets, sem = refs[:6], refs[6:12], refs[12]
    copies = [pltpu.make_async_copy(a, b, sem.at[i]) for i, (a, b) in enumerate(zip(sources, targets))]
    for copy in copies:
        copy.start()
    for copy in copies:
        copy.wait()


def per_device(dims, up_pre, gate_value, out_cotangent, down_weight, conv_weight, conv_bias):
    nx, ny, nz = dims
    tokens, width = up_pre.shape
    depth, rows = out_cotangent.shape[1], down_weight.shape[0]
    hx, hz = nx // 2, nz // 2
    y_offs = ring_offsets(ny)
    n_rel = max(1, len([o for o in y_offs if o in RELAY]))
    n_fin = len([o for o in y_offs if o not in RELAY])
    vmem, dma = pltpu.VMEM, pltpu.SemaphoreType.DMA
    scratch = [
        vmem((nx, 2, 2, tokens // 2, depth), BF16),
        vmem((nz, ny, rows, width), BF16),
        vmem((tokens + 8, width), F32),
        vmem((tokens, width), F32),
        vmem((tokens, width), F32),
        vmem((tokens, width), BF16),
        vmem((2, tokens // 2, width), F32),
        vmem((tokens + 8, width), F32),
        vmem((nx, ny, rows, width), F32),
        vmem((nx, ny, rows, width), BF16),
        vmem((nx, n_rel, rows, width), BF16),
        vmem((nx, 2, rows, width), BF16),
        vmem((nx, n_fin, rows, width), BF16),
        vmem((nx, rows, width), BF16),
        vmem((nz - 1, rows, width), BF16),
        vmem((rows, width), F32),
        vmem((16, width), BF16),
        vmem((8, width), F32),
        vmem((ny, 4, width), F32),
        vmem((nz, 4, width), F32),
        vmem((ny, 1, width), F32),
        vmem((nz, 1, width), F32),
        vmem((tokens, width), BF16),
        vmem((tokens, width), BF16),
        vmem((3, width), F32),
        vmem((1, width), F32),
        dma((7,)),
        dma((1,)), dma((2, hx, 2)),
        dma((1,)), dma((hx + 1,)),
        dma((1,)), dma((1,)),
        dma((1,)), dma((2, hz, 2)),
        dma((1,)), dma((nx,)),
        dma((1,)), dma((nx,)),
        dma((1,)), dma((1,)),
        dma((2,)), dma((2,)),
        dma((4,)), dma((4,)),
    ]
    spec = pl.BlockSpec(memory_space=pltpu.VMEM)
    hbm = pl.BlockSpec(memory_space=pltpu.HBM)
    shapes = (
        jax.ShapeDtypeStruct((tokens, width), BF16),
        jax.ShapeDtypeStruct((tokens, width), BF16),
        jax.ShapeDtypeStruct((rows, width), F32),
        jax.ShapeDtypeStruct((3, width), F32),
        jax.ShapeDtypeStruct((1, width), F32),
        jax.ShapeDtypeStruct((1, width), F32),
    )
    results = pl.pallas_call(
        functools.partial(kernel, dims),
        out_shape=shapes,
        in_specs=[hbm] * 6,
        out_specs=(spec,) * 6,
        scratch_shapes=scratch,
        compiler_params=pltpu.CompilerParams(
            collective_id=0, has_side_effects=True, vmem_limit_bytes=40 * 1024 * 1024
        ),
    )(*[pltpu.with_memory_space_constraint(v, pltpu.HBM) for v in (up_pre, gate_value, out_cotangent, down_weight, conv_weight, conv_bias[None])])
    up_grad, gate_grad, weight_grad, tap_grad, bias_grad, unit_norms = pl.pallas_call(
        store,
        out_shape=shapes,
        in_specs=[spec] * 6,
        out_specs=(hbm,) * 6,
        scratch_shapes=[dma((6,))],
        compiler_params=pltpu.CompilerParams(vmem_limit_bytes=4 * 1024 * 1024),
    )(*results)
    return up_grad, gate_grad, weight_grad, tap_grad, bias_grad[0], unit_norms[0]


def solution(mesh):
    nx = mesh.shape["tp"] // 2
    dims = (nx, mesh.shape["fs"] // nx, nx)
    return jax.shard_map(
        functools.partial(per_device, dims),
        mesh=mesh,
        in_specs=(P("fs", "tp"), P("fs", "tp"), P("fs", "tp"), P("fs", "tp"), P(None, "tp"), P("tp")),
        out_specs=(P("fs", "tp"), P("fs", "tp"), P("fs", "tp"), P(None, "tp"), P("tp"), P("tp")),
        check_vma=False,
    )
```

time: 84.5 us -> 66.7 us (0.79)
  the two profiles are of different devices: /device:TPU:2 before, /device:TPU:4 now
where the time goes in v2:
time: 66.7 us; the launch traced here: 66.5 us
  Pallas kernels  65.9 us (99%)
    pallas_call x1, Pallas kernels, per_device(): pl.pallas_call(functools.partial(kernel, dims), out_shape=shapes, in_spec...  65 us

profile of v2, /device:TPU:4, one launch (start us, length us, event | category | flops | bytes accessed | tf_op | source)
XLA Modules:
  0.0 66.5 jit_solution(11436407627578857446)
XLA Ops:
  0.6 65.0 %shard_map.109 = (bf16[768,256]{1,0:T(8,128)(2,1)S(1)}, bf16[768,256]{1,0:T(8,128)(2,1)S(1)}, f32[32,256]{1,0:T(8,128)S(1)}, f32[3,256]{1,0:T(4,128)S(1)}, f32[1,256]{1,0:T(1,128)S(1)}, /*index=5*/f32[1,256]{1,0:T(1,128)S(1)}) custom-call(bf16[768,256]{1,0:T(8,128)(2,1)} %up_in.1, bf16[768,256]{1,0:T(8,128)(2,1)} %gate_in.1, bf16[768,128]{1,0:T(8,128)(2,1)} %cot_in.1, ...), custom_call_target="tpu_custom_call" | custom-call | tf_op jit(solution)/shard_map/pallas_call | solution.py:442
  65.6 0.9 %shard_map.110 = (bf16[768,256]{1,0:T(8,128)(2,1)}, bf16[768,256]{1,0:T(8,128)(2,1)}, f32[32,256]{1,0:T(8,128)}, f32[3,256]{1,0:T(4,128)}, f32[1,256]{1,0:T(1,128)}, /*index=5*/f32[1,256]{1,0:T(1,128)}) custom-call(bf16[768,256]{1,0:T(8,128)(2,1)S(1)} %get-tuple-element.18.refs_0_, bf16[768,256]{1,0:T(8,128)(2,1)S(1)} %get-tuple-element.19.refs_1_, ...), custom_call_target="tpu_custom_call" | custom-call | tf_op jit(solution)/shard_map/pallas_call | solution.py:452
